TPU v7x, 512 devices: a whole 4x8x8 slice. The times are simulated.
512 devices in a mesh: sp: 64 (over z, y), fs: 4 (over x), tp: 2 (over core).
Axes of the slice: x: 4, y: 8, z: 8, core: 2. Of those that a mesh axis runs over, the one named last changes fastest.
Arguments:
- tokens: bfloat16 [4, 8192, 2048], P('fs', ('sp', 'tp')), may hold values from -6 to 6
- norm_gain: float32 [2048], replicated, may hold values from 0.1 to 1.9
- gla_query_weight: bfloat16 [2048, 512], P('sp', 'tp'), may hold values from -0.125 to 0.125
- gla_key_weight: bfloat16 [2048, 512], P('sp', 'tp'), may hold values from -0.125 to 0.125
- gla_value_weight: bfloat16 [2048, 1024], P('sp', 'tp'), may hold values from -0.125 to 0.125
- decay_down: bfloat16 [2048, 32], P('sp'), may hold values from -0.125 to 0.125
- decay_up: bfloat16 [32, 512], P(None, 'tp'), may hold values from -1 to 1
- decay_bias: float32 [512], P('tp'), may hold values from 0.5 to 12
- head_gain: float32 [128], replicated, may hold values from 0.1 to 1.9
- window_query_weight: bfloat16 [2048, 1024], P('sp', 'tp'), may hold values from -3 to 3
- window_key_weight: bfloat16 [2048, 256], P('sp', 'tp'), may hold values from -3 to 3
- window_value_weight: bfloat16 [2048, 256], P('sp', 'tp'), may hold values from -0.125 to 0.125
- sink_logit: float32 [16], P('tp'), may hold values from 3 to 7
- gla_output_weight: bfloat16 [1024, 2048], P('tp', 'sp'), may hold values from -0.125 to 0.125
- window_output_weight: bfloat16 [1024, 2048], P('tp', 'sp'), may hold values from -0.125 to 0.125
Outputs:
- mixed: bfloat16 [4, 8192, 2048], P('fs', ('sp', 'tp'))
All inputs are finite; a program needn't handle non-finite values.
Results may differ from a plain program's by a relative error of at most 0.013.
Values may be sent and summed in bfloat16 or wider, within the bound.
A program may use at most 64 MiB of HBM per device.

v0:
```python
import jax
import jax.numpy as jnp
from jax import lax
from jax.sharding import Mesh
from jax.sharding import PartitionSpec as P

KEY_DIM = 64
VALUE_DIM = 128
HEAD_DIM = 64
WINDOW = 128
SPAN = 64
SP = ("sp_0", "sp_1")
SP_TP = ("sp_0", "sp_1", "tp")
GROUP = ("fs", "tp")
EPS = 1e-06
SOFTMAX_TEMPER = 16.0
HIGH = lax.Precision.HIGHEST


def rms_rows(values, gain):
    mean_square = jnp.mean(values * values, axis=-1, keepdims=True)
    return values * lax.rsqrt(mean_square + EPS) * gain


def own_part(value, at, size, dim):
    return lax.dynamic_slice_in_dim(value, at * size, size, axis=dim)


def combine(earlier, later):
    return (later[1][..., None] * earlier[0] + later[0], earlier[1] * later[1])


def carried_in(value):
    start = (jnp.zeros_like(value[0]), jnp.ones_like(value[1]))
    before, subtotal = (start, value)
    for axis in ("sp_1", "sp_0"):
        peers, place = (lax.axis_size(axis), lax.axis_index(axis))
        both = jnp.concatenate(
            [subtotal[0], jnp.broadcast_to(subtotal[1][..., None], subtotal[0].shape[:-1] + (1,))],
            -1,
        )
        pieces = lax.all_gather(both, axis)
        inside, subtotal = (start, start)
        for k in range(peers):
            subtotal = combine(subtotal, (pieces[k, ..., :-1], pieces[k, ..., -1]))
            inside = jax.tree.map(lambda n, o: jnp.where(k < place, n, o), subtotal, inside)
        before = combine(inside, before)
    return before[0]


def per_device(
    tokens,
    norm_gain,
    gla_query_weight,
    gla_key_weight,
    gla_value_weight,
    decay_down,
    decay_up,
    decay_bias,
    head_gain,
    window_query_weight,
    window_key_weight,
    window_value_weight,
    sink_logit,
    gla_output_weight,
    window_output_weight,
):
    x = lax.axis_index("fs")
    rows = lax.all_gather(tokens[0], GROUP, axis=0, tiled=True)
    w_in = jnp.concatenate(
        [
            own_part(gla_query_weight, x, 64, 1),
            own_part(gla_key_weight, x, 64, 1),
            own_part(gla_value_weight, x, 128, 1),
            own_part(window_query_weight, x, 128, 1),
            own_part(window_key_weight, x // 2, 64, 1),
            own_part(window_value_weight, x // 2, 64, 1),
            decay_down,
        ],
        axis=1,
    )
    w_in = lax.all_gather(w_in, SP, axis=0, tiled=True)
    w_out = jnp.concatenate(
        [own_part(gla_output_weight, x, 128, 0), own_part(window_output_weight, x, 128, 0)], axis=0
    ).T
    w_out = lax.all_gather(w_out, SP, axis=0, tiled=True)
    normed = rms_rows(rows.astype(jnp.float32), norm_gain).astype(jnp.bfloat16)
    proj = jnp.dot(normed, w_in, preferred_element_type=jnp.float32).astype(jnp.bfloat16)
    seqs = 4
    spans = rows.shape[0] // seqs // SPAN
    gate = jnp.dot(proj[:, 512:], own_part(decay_up, x, 64, 1), preferred_element_type=jnp.float32)
    log_rate = jax.nn.log_sigmoid(gate + own_part(decay_bias, x, 64, 0)) / SOFTMAX_TEMPER

    def blocks(v):
        return v.astype(jnp.float32).reshape(seqs, spans, SPAN, -1)

    q, k, v = (
        blocks(proj[:, :64]) * KEY_DIM ** (-0.5),
        blocks(proj[:, 64:128]),
        blocks(proj[:, 128:256]),
    )
    within = jnp.cumsum(blocks(log_rate), axis=2)
    block_total = within[:, :, -1]
    q_dec = q * jnp.exp(within)
    k_dec = k * jnp.exp(-within)
    k_end = k * jnp.exp(block_total[:, :, None] - within)
    scores = jnp.einsum("snid,snjd->snij", q_dec, k_dec, precision=HIGH)
    scores = jnp.where(jnp.tril(jnp.ones((SPAN, SPAN), bool)), scores, 0.0)
    local_out = jnp.einsum("snij,snje->snie", scores, v, precision=HIGH)
    update = jnp.einsum("snjd,snje->snde", k_end, v, precision=HIGH)
    decay = jnp.exp(block_total)
    last_state = decay[:, 1, :, None] * update[:, 0] + update[:, 1]
    incoming = carried_in((last_state, decay[:, 0] * decay[:, 1]))
    entering = jnp.stack([incoming, decay[:, 0, :, None] * incoming + update[:, 0]], axis=1)
    wq = proj[:, 256:384].reshape(seqs, WINDOW, 2, HEAD_DIM)
    wkv = proj[:, 384:512].reshape(seqs, WINDOW, 2 * HEAD_DIM)
    ny, nz = (lax.axis_size("sp_1"), lax.axis_size("sp_0"))
    n = ny * nz
    edge = lax.ppermute(wkv, SP, [(i, i + 1) for i in range(n - 1)])
    band = jnp.concatenate([edge, wkv], axis=1)
    s = jnp.einsum("sqhd,skd->shqk", wq, band[..., :64], preferred_element_type=jnp.float32)
    s = s * HEAD_DIM ** (-0.5)
    dist = jnp.arange(WINDOW)[:, None] + WINDOW - jnp.arange(2 * WINDOW)[None]
    ok = (dist >= 0) & (dist < WINDOW)
    ok = ok & ((lax.axis_index(SP) > 0) | (jnp.arange(2 * WINDOW)[None] >= WINDOW))
    s = jnp.where(ok, s, -1e30)
    sink = own_part(sink_logit, x, 2, 0)[None, :, None, None]
    top = jnp.maximum(jnp.max(s, -1, keepdims=True), sink)
    e = jnp.exp(s - top)
    den = jnp.sum(e, -1, keepdims=True) + jnp.exp(sink - top)
    att = jnp.einsum(
        "shqk,skd->sqhd",
        (e / den).astype(jnp.bfloat16),
        band[..., 64:],
        preferred_element_type=jnp.float32,
    ).astype(jnp.bfloat16)
    gla_out = local_out + jnp.einsum("snid,snde->snie", q_dec, entering, precision=HIGH)
    hidden = rms_rows(gla_out, head_gain).astype(jnp.bfloat16).reshape(-1, VALUE_DIM)
    hidden = jnp.concatenate([hidden, att.reshape(-1, 128)], axis=1)
    total = jnp.einsum("rk,nk->rn", hidden, w_out, preferred_element_type=jnp.float32)
    total = total.astype(jnp.bfloat16).reshape(8, -1, total.shape[1])
    arrived = lax.all_to_all(total, GROUP, split_axis=0, concat_axis=0, tiled=True)
    return arrived.astype(jnp.float32).sum(axis=0).astype(jnp.bfloat16)[None]


def solution(mesh):
    split = Mesh(
        mesh.devices.reshape(8, 8, mesh.shape["fs"], mesh.shape["tp"]), ("sp_0", "sp_1", "fs", "tp")
    )
    return jax.shard_map(
        per_device,
        mesh=split,
        in_specs=(
            P("fs", SP_TP, None),
            P(),
            P(SP, "tp"),
            P(SP, "tp"),
            P(SP, "tp"),
            P(SP, None),
            P(None, "tp"),
            P("tp"),
            P(),
            P(SP, "tp"),
            P(SP, "tp"),
            P(SP, "tp"),
            P("tp"),
            P("tp", SP),
            P("tp", SP),
        ),
        out_specs=P("fs", SP_TP, None),
        check_vma=False,
    )
```

profile of v0, /device:TPU:1, one launch (start us, length us, event | category | flops | bytes accessed | tf_op | source)
XLA Modules:
  0.0 351.1 jit_solution(2613073268380290763)
XLA Ops:
  6.5 0.7 all-gather.13.cloned.1.call-update
  7.3 0.8 constant_dynamic-slice_fusion.2
  8.1 0.8 constant_dynamic-slice_fusion.6
  8.9 0.7 constant_dynamic-slice_fusion.4
  9.6 1.4 concatenate.18
  11.1 0.8 dynamic_slice.40
  11.9 34.1 %all-gather.13.cloned.1.call-done = bf16[1,512,2048]{2,1,0:T(8,128)(2,1)} async-done(((bf16[1,64,2048]{2,1,0:T(8,128)(2,1)}), bf16[1,512,2048]{2,1,0:T(8,128)(2,1)}) %all-gather.13.cloned.1.call-update) | async-done | bytes 2097168 | tf_op jit(solution)/shard_map/all_gather | solution.py:69
  46.0 2.2 fusion
  48.2 81.3 %all-gather.9.cloned.1.call-done = bf16[2048,544]{1,0:T(8,128)(2,1)} async-done(((bf16[32,544]{1,0:T(8,128)(2,1)}), bf16[2048,544]{1,0:T(8,128)(2,1)}) %all-gather.9.cloned.1.call-update) | async-done | bytes 2228240 | tf_op jit(solution)/shard_map/all_gather | solution.py:82
  129.5 3.2 fusion.10
  132.8 0.8 copy-done.3
  134.7 0.4 fusion.20
  135.3 0.7 pad_maximum_fusion
  136.1 40.0 %all-gather.15.cloned.1.call-done = f32[32,64,129]{2,1,0:T(8,128)} async-done(((f32[4,64,129]{2,1,0:T(8,128)}), f32[32,64,129]{2,1,0:T(8,128)}) %all-gather.15.cloned.1.call-update) | async-done | bytes 1056784 | tf_op jit(solution)/shard_map/all_gather | solution.py:42
  176.1 1.6 slice_reduce_fusion.7
  177.7 1.6 bitcast_add_fusion.9
  179.4 0.7 pad_maximum_fusion.1
  180.2 0.7 constant_dynamic-slice_fusion
  180.9 0.6 maximum_bitcast_fusion
  181.8 0.9 convert_multiply_fusion.2
  182.8 2.7 collective-permute-start
  185.5 0.6 convolution_select_fusion
  186.4 1.0 collective-permute-done
  187.5 0.4 fusion.63
  188.6 34.4 %all-gather.17.cloned.1.call-done = f32[32,64,129]{2,1,0:T(8,128)} async-done(((f32[4,64,129]{2,1,0:T(8,128)}), f32[32,64,129]{2,1,0:T(8,128)}) %all-gather.17.cloned.1.call-update) | async-done | bytes 1056784 | tf_op jit(solution)/shard_map/all_gather | solution.py:42
  223.1 1.6 slice_reduce_fusion.6
  224.7 2.0 bitcast_add_fusion
  226.7 0.5 multiply_reduce_fusion
  227.5 78.2 %all-gather.11.cloned.1.call-done = bf16[2048,256]{1,0:T(8,128)(2,1)} async-done(((bf16[32,256]{1,0:T(8,128)(2,1)}), bf16[2048,256]{1,0:T(8,128)(2,1)}) %all-gather.11.cloned.1.call-update) | async-done | bytes 1048592 | tf_op jit(solution)/shard_map/all_gather | solution.py:86
  305.7 2.0 convolution_convert_fusion
  307.7 35.7 %all_to_all.5 = bf16[8,64,2048]{2,1,0:T(8,128)(2,1)S(1)} all-to-all(bf16[8,64,2048]{2,1,0:T(8,128)(2,1)S(1)} %bitcast.222), channel_id=1, replica_groups=mesh['sp_0'=8,'sp_1'=8,'fs'=4,'tp'=2] {'fs','tp'}, dimensions={0} | all-to-all | bytes 4194304 | tf_op jit(solution)/shard_map/all_to_all | solution.py:142
  343.4 1.1 reduce_sum.42
  (56 shorter events, 3.2 us)
Async XLA Ops:
  6.5 127.0 %copy-start = (bf16[32,256]{1,0:T(8,128)(2,1)S(1)}, bf16[32,256]{1,0:T(8,128)(2,1)}, u32[]{:S(2)}) copy-start(bf16[32,256]{1,0:T(8,128)(2,1)} %param.21) | copy-start | bytes 49156
  6.5 123.0 %copy-start.5 = (f32[2048]{0:T(1024)S(1)}, f32[2048]{0:T(1024)}, u32[]{:S(2)}) copy-start(f32[2048]{0:T(1024)} %param.16) | copy-start | bytes 24580
  6.5 39.5 %all-gather.13.cloned.1.call-start = ((), (), s32[]{:S(2)}) async-start(), calls=%async_computation.3 | async-start | bytes 2359296 | tf_op jit(solution)/shard_map/all_gather | solution.py:69
  7.3 122.2 %all-gather.9.cloned.1.call-start = ((), (), s32[]{:S(2)}) async-start(), calls=%async_computation.1 | async-start | bytes 2662400 | tf_op jit(solution)/shard_map/all_gather | solution.py:82
  11.1 165.0 %all-gather.15.cloned.1.call-start = ((), (), s32[]{:S(2)}) async-start(), calls=%async_computation.4 | async-start | bytes 2359296 | tf_op jit(solution)/shard_map/all_gather | solution.py:42
  46.0 83.5 %copy-start.2 = (bf16[1,512,2048]{2,1,0:T(8,128)(2,1)S(1)}, bf16[1,512,2048]{2,1,0:T(8,128)(2,1)}, u32[]{:S(2)}) copy-start(bf16[1,512,2048]{2,1,0:T(8,128)(2,1)} %all-gather.13.cloned.1.call-done) | copy-start | bytes 6291460
  132.8 0.8 copy-start.3
  135.2 46.5 %copy-start.6 = (f32[8]{0:T(128)S(1)}, f32[8]{0:T(128)}, u32[]{:S(2)}) copy-start(f32[8]{0:T(128)} %param.27) | copy-start | bytes 100
  136.0 87.1 %all-gather.17.cloned.1.call-start = ((), (), s32[]{:S(2)}) async-start(), calls=%async_computation.5 | async-start | bytes 2359296 | tf_op jit(solution)/shard_map/all_gather | solution.py:42
  180.1 125.6 %all-gather.11.cloned.1.call-start = ((), (), s32[]{:S(2)}) async-start(), calls=%async_computation.2 | async-start | bytes 1064960 | tf_op jit(solution)/shard_map/all_gather | solution.py:86
  182.8 4.6 %collective-permute-start = (bf16[4,128,128]{1,2,0:T(8,128)(2,1)S(1)}, bf16[4,128,128]{1,2,0:T(8,128)(2,1)S(1)}, u32[]{:S(2)}, u32[]{:S(2)}) collective-permute-start(bf16[4,128,128]{1,2,0:T(8,128)(2,1)S(1)} %bitcast.238), channel_id=1, source_target_pairs={{0,8},{8,16},{16,24},{24,32},{32,40},{40,48},{48,56},{56,64},{64,7... | collective-permute-start | bytes 393224 | tf_op jit(solution)/shard_map/ppermute | solution.py:119
  188.2 36.6 %copy-start.1 = (f32[32,64,129]{2,1,0:T(8,128)S(1)}, f32[32,64,129]{2,1,0:T(8,128)}, u32[]{:S(2)}) copy-start(f32[32,64,129]{2,1,0:T(8,128)} %all-gather.15.cloned.1.call-done) | copy-start | bytes 3170308
  224.7 2.5 copy-start.4
Sparse Core Ops, SparseCore 0:
  9.5 36.4 all-gather.12
  49.0 80.4 all-gather.8
  136.1 39.8 all-gather.14
  180.2 42.7 all-gather.16
  226.0 79.6 all-gather.10
where the time goes:
time: 352 us; the launch traced here: 351 us
  waiting for transfers between devices  270 us (77%)
  blocking collectives  35.7 us (10%)
  other arithmetic  14.1 us (4%)
  between operations  13.5 us (4%)
  matrix products  8.02 us (2%)
  local copies, waits for them, and re-layouts  7.07 us (2%)
    all_gather x1, waiting for transfers between devices, per_device(): w_in = lax.all_gather(w_in, SP, axis=0, tiled=True)  81.3 us
    all_gather x1, waiting for transfers between devices, per_device(): w_out = lax.all_gather(w_out, SP, axis=0, tiled=True)  78.2 us
    all_gather x2, waiting for transfers between devices, carried_in(): pieces = lax.all_gather(both, axis)  74.4 us
    all_to_all x1, blocking collectives, per_device(): lax.all_to_all(total, GROUP, split_axis=0, concat_axis=0, tiled=True)  35.7 us
    all_gather x1, waiting for transfers between devices, per_device(): rows = lax.all_gather(tokens[0], GROUP, axis=0, tiled=True)  34.1 us
  transfers between devices with their start and end apart: 6, of which 6 were waited for; matrix products, arithmetic and copies ran while one was open for 4% of the time, Pallas kernels for 0%

commit v1 on v0

--- a/solution.py
+++ b/solution.py
@@ -83,7 +83,9 @@
     w_out = jnp.concatenate(
         [own_part(gla_output_weight, x, 128, 0), own_part(window_output_weight, x, 128, 0)], axis=0
     ).T
-    w_out = lax.all_gather(w_out, SP, axis=0, tiled=True)
+    w_out = jnp.concatenate(
+        lax.all_to_all(jnp.stack([w_out] * lax.axis_size(SP)), SP, 0, 0), axis=0
+    )
     normed = rms_rows(rows.astype(jnp.float32), norm_gain).astype(jnp.bfloat16)
     proj = jnp.dot(normed, w_in, preferred_element_type=jnp.float32).astype(jnp.bfloat16)
     seqs = 4

time: 352 us -> 289 us (0.82)
  waiting for transfers between devices: 270 us -> 199 us
  starting transfers between devices: 2.84 us -> 11.4 us
    all_gather x1 -> x0, waiting for transfers between devices: 78.2 us -> none  [per_device(): w_out = lax.all_gather(w_out, SP, axis=0, tiled=True)]
    all_to_all x0 -> x1, starting transfers between devices: none -> 8.31 us  [per_device(): lax.all_to_all(jnp.stack([w_out] * lax.axis_size(SP)), SP, 0, 0)]
    all_gather x2, waiting for transfers between devices: 74.4 us -> 82.5 us  [carried_in(): pieces = lax.all_gather(both, axis)]
  transfers between devices with their start and end apart: 6 -> 6, of which waited for: 6 -> 4; matrix products, arithmetic and copies ran while one was open for 4% -> 7% of each run, Pallas kernels for 0% -> 0%
where the time goes in v1:
time: 289 us; the launch traced here: 288 us
  waiting for transfers between devices  199 us (69%)
  blocking collectives  35 us (12%)
  other arithmetic  13.9 us (5%)
  between operations  13.7 us (5%)
  starting transfers between devices  11.4 us (4%)
  local copies, waits for them, and re-layouts  8.17 us (3%)
  matrix products  7.52 us (3%)
    all_gather x2, waiting for transfers between devices, carried_in(): pieces = lax.all_gather(both, axis)  82.5 us
    all_gather x1, waiting for transfers between devices, per_device(): w_in = lax.all_gather(w_in, SP, axis=0, tiled=True)  81.3 us
    all_to_all x1, blocking collectives, per_device(): lax.all_to_all(total, GROUP, split_axis=0, concat_axis=0, tiled=True)  35 us
    all_gather x1, waiting for transfers between devices, per_device(): rows = lax.all_gather(tokens[0], GROUP, axis=0, tiled=True)  34.1 us
    all_to_all x1, starting transfers between devices, per_device(): lax.all_to_all(jnp.stack([w_out] * lax.axis_size(SP)), SP, 0, 0)  8.31 us
  transfers between devices with their start and end apart: 6, of which 4 were waited for; matrix products, arithmetic and copies ran while one was open for 7% of the time, Pallas kernels for 0%

profile of v1, /device:TPU:1, one launch (start us, length us, event | category | flops | bytes accessed | tf_op | source)
XLA Modules:
  0.0 288.3 jit_solution(2630206554834140843)
XLA Ops:
  6.5 0.7 all-gather.10.cloned.1.call-update
  7.3 0.8 constant_dynamic-slice_fusion.2
  8.1 0.8 constant_dynamic-slice_fusion.6
  8.9 0.7 constant_dynamic-slice_fusion.4
  9.6 1.4 concatenate.18
  11.1 0.8 dynamic_slice.40
  11.9 34.1 %all-gather.10.cloned.1.call-done = bf16[1,512,2048]{2,1,0:T(8,128)(2,1)} async-done(((bf16[1,64,2048]{2,1,0:T(8,128)(2,1)}), bf16[1,512,2048]{2,1,0:T(8,128)(2,1)}) %all-gather.10.cloned.1.call-update) | async-done | bytes 2097168 | tf_op jit(solution)/shard_map/all_gather | solution.py:69
  46.0 2.2 fusion
  48.2 81.3 %all-gather.8.cloned.1.call-done = bf16[2048,544]{1,0:T(8,128)(2,1)} async-done(((bf16[32,544]{1,0:T(8,128)(2,1)}), bf16[2048,544]{1,0:T(8,128)(2,1)}) %all-gather.8.cloned.1.call-update) | async-done | bytes 2228240 | tf_op jit(solution)/shard_map/all_gather | solution.py:82
  129.5 3.2 %fusion.10 = bf16[512,544]{0,1:T(8,128)(2,1)S(1)} fusion(bf16[2048,544]{1,0:T(8,128)(2,1)} %all-gather.8.cloned.1.call-done, bf16[1,512,2048]{2,1,0:T(8,128)(2,1)S(1)} %copy-done.4, f32[2048]{0:T(1024)S(1)} %copy-done.16, f32[512]{0:T(512)S(1)} %add_rsqrt_fusion.1), kind=kOutput, calls=%fused_computation.13 | convolution fusion | flops 1145323520 | bytes 4892672 | tf_op jit(solution)/shard_map/dot_general | solution.py:90
  133.6 0.6 fusion.62
  134.6 0.4 fusion.20
  135.0 0.7 copy-done.5
  135.8 0.7 pad_maximum_fusion
  136.5 0.7 constant_dynamic-slice_fusion
  137.3 1.1 stack.5
  138.4 8.3 %all-to-all-start = ((bf16[64,32,256]{2,1,0:T(8,128)(2,1)}), bf16[64,32,256]{2,1,0:T(8,128)(2,1)S(1)}, u32[]{:S(2)}, u32[]{:S(2)}) async-start(bf16[64,32,256]{2,1,0:T(8,128)(2,1)} %stack.5), calls=%async_computation | async-start | bytes 2097152 | tf_op jit(solution)/shard_map/all_to_all | solution.py:87
  147.2 2.9 %collective-permute-start = (bf16[4,128,128]{1,2,0:T(8,128)(2,1)S(1)}, bf16[4,128,128]{1,2,0:T(8,128)(2,1)S(1)}, u32[]{:S(2)}, u32[]{:S(2)}) collective-permute-start(bf16[4,128,128]{1,2,0:T(8,128)(2,1)S(1)} %bitcast.240), channel_id=1, source_target_pairs={{0,8},{8,16},{16,24},{24,32},{32,40},{40,48},{48,56},{56,64},{64,7... | collective-permute-start | bytes 393224 | tf_op jit(solution)/shard_map/ppermute | solution.py:121
  150.2 46.2 %all-gather.12.cloned.1.call-done = f32[32,64,129]{2,1,0:T(8,128)} async-done(((f32[4,64,129]{2,1,0:T(8,128)}), f32[32,64,129]{2,1,0:T(8,128)}) %all-gather.12.cloned.1.call-update) | async-done | bytes 1056784 | tf_op jit(solution)/shard_map/all_gather | solution.py:42
  196.4 1.6 slice_reduce_fusion.7
  198.1 0.6 select_select_fusion
  198.7 1.6 bitcast_add_fusion.9
  200.3 0.7 pad_maximum_fusion.1
  201.1 0.6 convolution_select_fusion
  201.7 1.0 fusion.64
  204.0 36.2 %all-gather.14.cloned.1.call-done = f32[32,64,129]{2,1,0:T(8,128)} async-done(((f32[4,64,129]{2,1,0:T(8,128)}), f32[32,64,129]{2,1,0:T(8,128)}) %all-gather.14.cloned.1.call-update) | async-done | bytes 1056784 | tf_op jit(solution)/shard_map/all_gather | solution.py:42
  240.2 1.7 slice_reduce_fusion.6
  242.0 2.1 bitcast_add_fusion
  244.0 0.5 multiply_reduce_fusion
  244.9 0.8 convolution_convert_fusion
  245.6 35.0 %all_to_all.10 = bf16[8,64,2048]{2,1,0:T(8,128)(2,1)S(1)} all-to-all(bf16[8,64,2048]{2,1,0:T(8,128)(2,1)S(1)} %bitcast.223), channel_id=1, replica_groups=mesh['sp_0'=8,'sp_1'=8,'fs'=4,'tp'=2] {'fs','tp'}, dimensions={0} | all-to-all | bytes 4194304 | tf_op jit(solution)/shard_map/all_to_all | solution.py:144
  280.6 1.1 reduce_sum.42
  (78 shorter events, 3.3 us)
Async XLA Ops:
  6.5 126.3 %copy-start = (bf16[32,256]{1,0:T(8,128)(2,1)S(1)}, bf16[32,256]{1,0:T(8,128)(2,1)}, u32[]{:S(2)}) copy-start(bf16[32,256]{1,0:T(8,128)(2,1)} %param.21) | copy-start | bytes 49156
  6.5 123.0 %copy-start.16 = (f32[2048]{0:T(1024)S(1)}, f32[2048]{0:T(1024)}, u32[]{:S(2)}) copy-start(f32[2048]{0:T(1024)} %param.16) | copy-start | bytes 24580
  6.5 39.5 %all-gather.10.cloned.1.call-start = ((), (), s32[]{:S(2)}) async-start(), calls=%async_computation.3 | async-start | bytes 2359296 | tf_op jit(solution)/shard_map/all_gather | solution.py:69
  7.3 122.2 %all-gather.8.cloned.1.call-start = ((), (), s32[]{:S(2)}) async-start(), calls=%async_computation.2 | async-start | bytes 2662400 | tf_op jit(solution)/shard_map/all_gather | solution.py:82
  11.1 185.3 %all-gather.12.cloned.1.call-start = ((), (), s32[]{:S(2)}) async-start(), calls=%async_computation.4 | async-start | bytes 2359296 | tf_op jit(solution)/shard_map/all_gather | solution.py:42
  46.0 83.5 %copy-start.4 = (bf16[1,512,2048]{2,1,0:T(8,128)(2,1)S(1)}, bf16[1,512,2048]{2,1,0:T(8,128)(2,1)}, u32[]{:S(2)}) copy-start(bf16[1,512,2048]{2,1,0:T(8,128)(2,1)} %all-gather.10.cloned.1.call-done) | copy-start | bytes 6291460
  135.0 0.7 copy-start.5
  135.8 11.0 %copy-start.17 = (f32[8]{0:T(128)S(1)}, f32[8]{0:T(128)}, u32[]{:S(2)}) copy-start(f32[8]{0:T(128)} %param.27) | copy-start | bytes 100
  138.4 106.5 %all-to-all-start = ((bf16[64,32,256]{2,1,0:T(8,128)(2,1)}), bf16[64,32,256]{2,1,0:T(8,128)(2,1)S(1)}, u32[]{:S(2)}, u32[]{:S(2)}) async-start(bf16[64,32,256]{2,1,0:T(8,128)(2,1)} %stack.5), calls=%async_computation | async-start | bytes 2097152 | tf_op jit(solution)/shard_map/all_to_all | solution.py:87
  146.7 93.5 %all-gather.14.cloned.1.call-start = ((), (), s32[]{:S(2)}) async-start(), calls=%async_computation.5 | async-start | bytes 2359296 | tf_op jit(solution)/shard_map/all_gather | solution.py:42
  147.2 54.5 %copy-start.2 = (f32[512,64]{1,0:T(8,128)}, f32[512,64]{1,0:T(8,128)S(1)}, u32[]{:S(2)}) copy-start(f32[512,64]{1,0:T(8,128)S(1)} %copy.214) | copy-start | bytes 393220
  147.2 55.4 %collective-permute-start = (bf16[4,128,128]{1,2,0:T(8,128)(2,1)S(1)}, bf16[4,128,128]{1,2,0:T(8,128)(2,1)S(1)}, u32[]{:S(2)}, u32[]{:S(2)}) collective-permute-start(bf16[4,128,128]{1,2,0:T(8,128)(2,1)S(1)} %bitcast.240), channel_id=1, source_target_pairs={{0,8},{8,16},{16,24},{24,32},{32,40},{40,48},{48,56},{56,64},{64,7... | collective-permute-start | bytes 393224 | tf_op jit(solution)/shard_map/ppermute | solution.py:121
  198.1 4.7 %copy-start.8 = (f32[4,64]{1,0:T(4,128)}, f32[4,64]{1,0:T(4,128)S(1)}, u32[]{:S(2)}) copy-start(f32[4,64]{1,0:T(4,128)S(1)} %get-tuple-element.14) | copy-start | bytes 3076
  198.1 4.7 %copy-start.9 = (f32[4,64]{1,0:T(4,128)}, f32[4,64]{1,0:T(4,128)S(1)}, u32[]{:S(2)}) copy-start(f32[4,64]{1,0:T(4,128)S(1)} %get-tuple-element.15) | copy-start | bytes 3076
  198.1 4.7 %copy-start.10 = (f32[4,64]{1,0:T(4,128)}, f32[4,64]{1,0:T(4,128)S(1)}, u32[]{:S(2)}) copy-start(f32[4,64]{1,0:T(4,128)S(1)} %get-tuple-element.16) | copy-start | bytes 3076
  198.1 4.7 %copy-start.11 = (f32[4,64]{1,0:T(4,128)}, f32[4,64]{1,0:T(4,128)S(1)}, u32[]{:S(2)}) copy-start(f32[4,64]{1,0:T(4,128)S(1)} %get-tuple-element.17) | copy-start | bytes 3076
  198.1 4.7 %copy-start.12 = (f32[4,64]{1,0:T(4,128)}, f32[4,64]{1,0:T(4,128)S(1)}, u32[]{:S(2)}) copy-start(f32[4,64]{1,0:T(4,128)S(1)} %get-tuple-element.18) | copy-start | bytes 3076
  198.1 4.7 %copy-start.13 = (f32[4,64]{1,0:T(4,128)}, f32[4,64]{1,0:T(4,128)S(1)}, u32[]{:S(2)}) copy-start(f32[4,64]{1,0:T(4,128)S(1)} %get-tuple-element.19) | copy-start | bytes 3076
  198.1 5.3 %copy-start.7 = (f32[4,64]{1,0:T(4,128)}, f32[4,64]{1,0:T(4,128)S(1)}, u32[]{:S(2)}) copy-start(f32[4,64]{1,0:T(4,128)S(1)} %get-tuple-element.13) | copy-start | bytes 3076
  198.7 4.1 %copy-start.14 = (f32[4,64]{1,0:T(4,128)}, f32[4,64]{1,0:T(4,128)S(1)}, u32[]{:S(2)}) copy-start(f32[4,64]{1,0:T(4,128)S(1)} %get-tuple-element.31) | copy-start | bytes 3076
  203.5 38.4 %copy-start.1 = (f32[32,64,129]{2,1,0:T(8,128)S(1)}, f32[32,64,129]{2,1,0:T(8,128)}, u32[]{:S(2)}) copy-start(f32[32,64,129]{2,1,0:T(8,128)} %all-gather.12.cloned.1.call-done) | copy-start | bytes 3170308
  240.2 3.8 %copy-start.3 = (f32[512,64]{1,0:T(8,128)S(1)}, f32[512,64]{1,0:T(8,128)}, u32[]{:S(2)}) copy-start(f32[512,64]{1,0:T(8,128)} %copy-done.2) | copy-start | bytes 393220
  240.2 3.8 %copy-start.6 = (f32[4,2,64,128]{3,2,1,0:T(8,128)S(1)}, f32[4,2,64,128]{3,2,1,0:T(8,128)}, u32[]{:S(2)}) copy-start(f32[4,2,64,128]{3,2,1,0:T(8,128)} %fusion.64) | copy-start | bytes 786436
  241.9 2.7 copy-start.15
Sparse Core Ops, SparseCore 0:
  9.5 36.4 all-gather.9
  49.0 80.4 all-gather.7
  136.7 59.6 all-gather.11
  201.2 38.9 all-gather.13
